TPU v7x, 32 devices: a whole 2x2x4 slice. The times are simulated.
32 devices in a mesh: fs: 8 (over z, x), tp: 4 (over y, core).
Axes of the slice: x: 2, y: 2, z: 4, core: 2. Of those that a mesh axis runs over, the one named last changes fastest.
Arguments:
- later_input: bfloat16 [4096, 2048], P(('fs', 'tp')), may hold values from -6 to 6
- saved_input: bfloat16 [4096, 2048], P(('fs', 'tp')), may hold values from -6 to 6
- cotangent: bfloat16 [4096, 3072], P('fs', 'tp'), may hold values from -6 to 6
- up_weight: bfloat16 [2048, 3072], P('fs', 'tp'), may hold values from -0.125 to 0.125
- gate_weight: bfloat16 [2048, 3072], P('fs', 'tp'), may hold values from -0.125 to 0.125
- up_taps: bfloat16 [3, 3072], replicated, may hold values from -3.5 to 3.5
- gate_taps: bfloat16 [3, 3072], replicated, may hold values from -3.5 to 3.5
- up_grad_sum: float32 [2048, 3072], P('fs', 'tp'), may hold values from -6 to 6
- gate_grad_sum: float32 [2048, 3072], P('fs', 'tp'), may hold values from -6 to 6
- up_taps_sum: float32 [3, 3072], replicated, may hold values from -6 to 6
- gate_taps_sum: float32 [3, 3072], replicated, may hold values from -6 to 6
Outputs:
- hidden: bfloat16 [4096, 3072], P('fs', 'tp')
- input_grad: bfloat16 [4096, 2048], P(('fs', 'tp'))
- new_up_sum: float32 [2048, 3072], P('fs', 'tp')
- new_gate_sum: float32 [2048, 3072], P('fs', 'tp')
- new_up_taps_sum: float32 [3, 3072], replicated
- new_gate_taps_sum: float32 [3, 3072], replicated
All inputs are finite; a program needn't handle non-finite values.
Results may differ from a plain program's by a relative error of at most 0.018.
Values may be sent and summed in bfloat16 or wider, within the bound.
A program may use at most 64 MiB of HBM per device.

v0:
```python
import jax
import jax.numpy as jnp
from jax import lax
from jax.sharding import PartitionSpec as P


def delayed(values, steps):
    zeros = jnp.zeros_like(values[:steps])
    return jnp.concatenate([zeros, values[:-steps]], axis=0)


def advanced(values, steps):
    zeros = jnp.zeros_like(values[:steps])
    return jnp.concatenate([values[steps:], zeros], axis=0)


def depthwise(values, taps):
    return taps[2] * values + taps[1] * delayed(values, 1) + taps[0] * delayed(values, 2)


def depthwise_back(grads, taps):
    return taps[2] * grads + taps[1] * advanced(grads, 1) + taps[0] * advanced(grads, 2)


def taps_grad(grads, values):
    return jnp.stack(
        [
            jnp.sum(grads * delayed(values, 2), axis=0),
            jnp.sum(grads * delayed(values, 1), axis=0),
            jnp.sum(grads * values, axis=0),
        ],
        axis=0,
    )


def make_term(rows_all, grads):
    return lax.dot_general(
        rows_all, grads, (((0,), (0,)), ((), ())), preferred_element_type=jnp.float32
    )


def shards(
    later_input,
    saved_input,
    cotangent,
    up_weight,
    gate_weight,
    up_taps,
    gate_taps,
    up_grad_sum,
    gate_grad_sum,
    up_taps_sum,
    gate_taps_sum,
):
    column_count = up_weight.shape[1]
    group_size = lax.axis_size("tp")
    offset = lax.axis_index("tp") * column_count
    tokens_all = later_input.shape[0] * lax.axis_size("fs") * group_size
    grad_scale = jnp.float32(tokens_all ** (-0.5))
    taps_both = jnp.concatenate(
        [
            lax.dynamic_slice_in_dim(up_taps, offset, column_count, 1),
            lax.dynamic_slice_in_dim(gate_taps, offset, column_count, 1),
        ],
        axis=1,
    ).astype(jnp.float32)
    weight_both = jnp.concatenate([up_weight, gate_weight], axis=1)
    later_rows = lax.all_gather(later_input, "tp", axis=0, tiled=True)
    saved_rows = lax.all_gather(saved_input, "tp", axis=0, tiled=True)
    shard_rows = lax.all_gather(weight_both, "fs", axis=0, tiled=True)
    proj_later = jnp.dot(later_rows, shard_rows, preferred_element_type=jnp.float32)
    proj_saved = jnp.dot(saved_rows, shard_rows, preferred_element_type=jnp.float32)
    conv_later = depthwise(proj_later.astype(jnp.bfloat16).astype(jnp.float32), taps_both)
    hidden = (jax.nn.silu(conv_later[:, column_count:]) * conv_later[:, :column_count]).astype(
        jnp.bfloat16
    )
    saved_proj = proj_saved.astype(jnp.bfloat16)
    saved_proj32 = saved_proj.astype(jnp.float32)
    conv_saved = depthwise(saved_proj32, taps_both)
    saved_up = conv_saved[:, :column_count]
    saved_gate = conv_saved[:, column_count:]
    sigmoid_gate = jax.nn.sigmoid(saved_gate)
    upstream = cotangent.astype(jnp.float32)
    grad_conv = jnp.concatenate(
        [
            upstream * jax.nn.silu(saved_gate),
            upstream * saved_up * sigmoid_gate * (1.0 + saved_gate * (1.0 - sigmoid_gate)),
        ],
        axis=1,
    )
    grad_proj = depthwise_back(grad_conv, taps_both).astype(jnp.bfloat16)
    taps_local = taps_grad(grad_conv, saved_proj32)
    total_cols = column_count * group_size
    taps_up_full = lax.dynamic_update_slice_in_dim(
        jnp.zeros((3, total_cols), jnp.float32), taps_local[:, :column_count], offset, 1
    )
    taps_gate_full = lax.dynamic_update_slice_in_dim(
        jnp.zeros((3, total_cols), jnp.float32), taps_local[:, column_count:], offset, 1
    )
    taps_up_total, taps_gate_total = lax.psum((taps_up_full, taps_gate_full), ("fs", "tp"))
    weight_grad = lax.psum_scatter(
        make_term(saved_rows, grad_proj).astype(jnp.bfloat16), "fs", scatter_dimension=0, tiled=True
    ).astype(jnp.float32)
    up_grad = weight_grad[:, :column_count]
    gate_grad = weight_grad[:, column_count:]
    partial_grad = lax.dot_general(
        grad_proj,
        lax.all_gather(weight_both, "fs", axis=0, tiled=True),
        (((1,), (1,)), ((), ())),
        preferred_element_type=jnp.float32,
    )
    input_grad = lax.psum_scatter(
        partial_grad.astype(jnp.bfloat16), "tp", scatter_dimension=0, tiled=True
    )
    new_up_sum = up_grad_sum + grad_scale * up_grad
    new_gate_sum = gate_grad_sum + grad_scale * gate_grad
    new_up_taps_sum = up_taps_sum + grad_scale * taps_up_total
    new_gate_taps_sum = gate_taps_sum + grad_scale * taps_gate_total
    return (hidden, input_grad, new_up_sum, new_gate_sum, new_up_taps_sum, new_gate_taps_sum)


def solution(mesh):
    return jax.shard_map(
        shards,
        mesh=mesh,
        in_specs=(
            P(("fs", "tp"), None),
            P(("fs", "tp"), None),
            P("fs", "tp"),
            P("fs", "tp"),
            P("fs", "tp"),
            P(),
            P(),
            P("fs", "tp"),
            P("fs", "tp"),
            P(),
            P(),
        ),
        out_specs=(P("fs", "tp"), P(("fs", "tp"), None), P("fs", "tp"), P("fs", "tp"), P(), P()),
        check_vma=False,
    )
```

profile of v0, /device:TPU:0, one launch (start us, length us, event | category | flops | bytes accessed | tf_op | source)
XLA Modules:
  0.0 459.7 jit_solution(4171032246797810518)
XLA Ops:
  7.2 0.7 all-gather.8.cloned.1.call-update
  8.0 2.0 pad_maximum_fusion.1
  10.1 0.7 all-gather.6.cloned.1.call-update
  10.8 1.2 copy.17
  12.0 0.7 constant_dynamic-slice_fusion
  12.8 22.1 %all-gather.8.cloned.1.call-done = bf16[512,2048]{1,0:T(8,128)(2,1)} async-done(((bf16[128,2048]{1,0:T(8,128)(2,1)}), bf16[512,2048]{1,0:T(8,128)(2,1)}) %all-gather.8.cloned.1.call-update) | async-done | bytes 2097168 | tf_op jit(solution)/shard_map/all_gather | solution.py:69
  34.9 101.5 %all-gather.4.cloned.1.call-done = bf16[2048,1536]{1,0:T(8,128)(2,1)} async-done(((bf16[256,1536]{1,0:T(8,128)(2,1)}), bf16[2048,1536]{1,0:T(8,128)(2,1)}) %all-gather.4.cloned.1.call-update) | async-done | bytes 6291472 | tf_op jit(solution)/shard_map/all_gather | solution.py:70
  136.3 6.2 %convert_bitcast_fusion = f32[512,1536]{0,1:T(8,128)S(1)} fusion(bf16[2048,1536]{1,0:T(8,128)(2,1)} %all-gather.4.cloned.1.call-done, bf16[512,2048]{1,0:T(8,128)(2,1)} %all-gather.8.cloned.1.call-done), kind=kOutput, calls=%fused_computation.9 | convolution fusion | flops 3222798336 | bytes 11534336 | tf_op jit(solution)/shard_map/dot_general | solution.py:72
  142.6 2.6 multiply_add_fusion
  145.3 0.9 fusion.4
  146.2 2.7 fusion.1
  149.0 2.6 fusion.2
  151.6 7.1 %all-gather.6.cloned.1.call-done = bf16[512,2048]{1,0:T(8,128)(2,1)} async-done(((bf16[128,2048]{1,0:T(8,128)(2,1)}), bf16[512,2048]{1,0:T(8,128)(2,1)}) %all-gather.6.cloned.1.call-update) | async-done | bytes 2097168 | tf_op jit(solution)/shard_map/all_gather | solution.py:68
  158.7 6.4 %convert_bitcast_fusion.1 = f32[512,1536]{0,1:T(8,128)S(1)} fusion(bf16[2048,1536]{1,0:T(8,128)(2,1)} %all-gather.4.cloned.1.call-done, bf16[512,2048]{1,0:T(8,128)(2,1)} %all-gather.6.cloned.1.call-done), kind=kOutput, calls=%fused_computation.10 | convolution fusion | flops 3222798336 | bytes 11534336 | tf_op jit(solution)/shard_map/dot_general | solution.py:71
  165.1 7.4 %multiply_reduce_fusion.2 = (f32[1536]{0:T(1024)S(1)}, f32[1536]{0:T(1024)S(1)}, f32[1536]{0:T(1024)S(1)}, bf16[512,1536]{0,1:T(8,128)(2,1)}, f32[512,1536]{0,1:T(8,128)}) fusion(f32[510,1536]{0,1:T(8,128)S(1)} %bitcast.20, f32[512,768]{0,1:T(8,128)S(1)} %copy-done.1, f32[512,768]{0,1:T(8,128)S(1)} %copy-done.3, f32[512,1536]{0,1:T(8,128)S(1)} %convert_bitcast_fusion, ...), kind=kLoop, calls=%fused_computation.13 | loop fusion | flops 14151168 | bytes 33011712 | tf_op jit(solution)/shard_map/reduce_sum | solution.py:28
  172.7 0.6 copy-done.13
  173.3 0.2 reduce-scatter.5.cloned.1.call-start
  173.6 8.2 %fusion = bf16[2048,1536]{0,1:T(8,128)(2,1)} fusion(bf16[512,1536]{0,1:T(8,128)(2,1)} %get-tuple-element.22, bf16[512,2048]{1,0:T(8,128)(2,1)} %all-gather.8.cloned.1.call-done), kind=kOutput, calls=%fused_computation.1 | convolution fusion | flops 3224371200 | bytes 9961472 | tf_op jit(solution)/shard_map/dot_general | solution.py:37
  181.9 1.3 copy-done.10
  183.2 7.6 %convolution_convert_fusion.1 = bf16[512,2048]{1,0:T(8,128)(2,1)} fusion(bf16[512,1536]{0,1:T(8,128)(2,1)S(1)} %copy-done.10, bf16[2048,1536]{1,0:T(8,128)(2,1)} %all-gather.4.cloned.1.call-done), kind=kOutput, calls=%fused_computation.17 | convolution fusion | flops 3222274048 | bytes 9961472 | tf_op jit(solution)/shard_map/dot_general | solution.py:106
  190.8 2.5 copy.19
  193.2 2.3 copy.20
  195.5 1.4 fusion.5
  196.9 2.4 copy.21
  199.3 97.3 %all-reduce.9.cloned.1.call-done = (f32[3,3072]{1,0:T(4,128)}, f32[3,3072]{1,0:T(4,128)}) async-done(((f32[3,3072]{1,0:T(4,128)}, f32[3,3072]{1,0:T(4,128)}), (f32[3,3072]{1,0:T(4,128)}, f32[3,3072]{1,0:T(4,128)})) %all-reduce.9.cloned.1.call-update) | async-done | bytes 73744 | tf_op jit(solution)/shard_map/psum | solution.py:100
  296.6 1.4 multiply_add_fusion.2
  298.0 1.4 multiply_add_fusion.3
  299.5 120.0 %reduce-scatter.5.cloned.1.call-done = bf16[256,1536]{0,1:T(8,128)(2,1)} async-done(((bf16[2048,1536]{0,1:T(8,128)(2,1)}), bf16[256,1536]{0,1:T(8,128)(2,1)}) %reduce-scatter.5.cloned.1.call-update) | async-done | bytes 786448 | tf_op jit(solution)/shard_map/reduce_scatter | solution.py:101
  419.5 1.2 convert_element_type.57
  421.0 1.1 copy.22
  422.1 1.1 copy.23
  423.3 29.6 %reduce-scatter.3.cloned.1.call-done = bf16[128,2048]{1,0:T(8,128)(2,1)} async-done(((bf16[512,2048]{1,0:T(8,128)(2,1)}), bf16[128,2048]{1,0:T(8,128)(2,1)}) %reduce-scatter.3.cloned.1.call-update) | async-done | bytes 524304 | tf_op jit(solution)/shard_map/reduce_scatter | solution.py:112
  (49 shorter events, 0.7 us)
Async XLA Ops:
  7.2 3.7 copy-start.11
  7.2 27.7 %all-gather.8.cloned.1.call-start = ((), (), s32[]{:S(2)}) async-start(), calls=%async_computation.4 | async-start | bytes 2621440 | tf_op jit(solution)/shard_map/all_gather | solution.py:69
  7.9 128.4 %all-gather.4.cloned.1.call-start = ((), (), s32[]{:S(2)}) async-start(), calls=%async_computation.2 | async-start | bytes 7077888 | tf_op jit(solution)/shard_map/all_gather | solution.py:70
  10.0 148.7 %all-gather.6.cloned.1.call-start = ((), (), s32[]{:S(2)}) async-start(), calls=%async_computation.3 | async-start | bytes 2621440 | tf_op jit(solution)/shard_map/all_gather | solution.py:68
  10.8 285.8 %all-reduce.9.cloned.1.call-start = ((), (), s32[]{:S(2)}) async-start(), calls=%async_computation.7 | async-start | bytes 196608 | tf_op jit(solution)/shard_map/psum | solution.py:100
  142.6 2.7 copy-start.9
  146.2 2.8 copy-start
  146.2 2.7 copy-start.2
  158.7 6.4 %copy-start.1 = (f32[512,768]{0,1:T(8,128)S(1)}, f32[512,768]{0,1:T(8,128)}, u32[]{:S(2)}) copy-start(f32[512,768]{0,1:T(8,128)} %copy-done) | copy-start | bytes 4718596
  158.7 6.4 %copy-start.3 = (f32[512,768]{0,1:T(8,128)S(1)}, f32[512,768]{0,1:T(8,128)}, u32[]{:S(2)}) copy-start(f32[512,768]{0,1:T(8,128)} %copy-done.2) | copy-start | bytes 4718596
  158.7 6.4 %copy-start.4 = (f32[511,1536]{0,1:T(8,128)S(1)}, f32[511,1536]{0,1:T(8,128)}, u32[]{:S(2)}) copy-start(f32[511,1536]{0,1:T(8,128)} %fusion.1) | copy-start | bytes 9418756
  158.7 6.4 %copy-start.5 = (f32[510,1536]{0,1:T(8,128)S(1)}, f32[510,1536]{0,1:T(8,128)}, u32[]{:S(2)}) copy-start(f32[510,1536]{0,1:T(8,128)} %fusion.2) | copy-start | bytes 9400324
  172.7 0.6 copy-start.13
  172.7 0.6 copy-start.12
  173.3 246.1 %reduce-scatter.5.cloned.1.call-start = ((), (), s32[]{:S(2)}) async-start(), calls=%async_computation.6 | async-start | bytes 7077888 | tf_op jit(solution)/shard_map/reduce_scatter | solution.py:101
  181.8 1.4 copy-start.10
  181.8 271.1 %reduce-scatter.3.cloned.1.call-start = ((), (), s32[]{:S(2)}) async-start(), calls=%async_computation.5 | async-start | bytes 2621440 | tf_op jit(solution)/shard_map/reduce_scatter | solution.py:112
  190.7 4.8 %copy-start.6 = (f32[512,1536]{0,1:T(8,128)S(1)}, f32[512,1536]{0,1:T(8,128)}, u32[]{:S(2)}) copy-start(f32[512,1536]{0,1:T(8,128)} %get-tuple-element.25) | copy-start | bytes 9437188
  195.5 101.1 %copy-start.14 = (f32[3,3072]{1,0:T(4,128)S(1)}, f32[3,3072]{1,0:T(4,128)}, u32[]{:S(2)}) copy-start(f32[3,3072]{1,0:T(4,128)} %param.21) | copy-start | bytes 110596
  195.5 102.5 %copy-start.15 = (f32[3,3072]{1,0:T(4,128)S(1)}, f32[3,3072]{1,0:T(4,128)}, u32[]{:S(2)}) copy-start(f32[3,3072]{1,0:T(4,128)} %param.20) | copy-start | bytes 110596
  196.9 223.8 %copy-start.7 = (f32[256,768]{0,1:T(8,128)S(1)}, f32[256,768]{0,1:T(8,128)}, u32[]{:S(2)}) copy-start(f32[256,768]{0,1:T(8,128)} %copy.19) | copy-start | bytes 2359300
  196.9 223.9 %copy-start.8 = (f32[256,768]{0,1:T(8,128)S(1)}, f32[256,768]{0,1:T(8,128)}, u32[]{:S(2)}) copy-start(f32[256,768]{0,1:T(8,128)} %copy.20) | copy-start | bytes 2359300
Sparse Core Ops, SparseCore 0:
  9.5 25.2 all-gather.7
  37.6 98.6 all-gather.3
  137.9 20.7 all-gather.5
  173.5 123.0 all-reduce.8
  300.0 119.3 reduce-scatter.4
  422.4 30.4 reduce-scatter.2
where the time goes:
time: 460 us
  waiting for transfers between devices  379 us (82%)
  matrix products  28.4 us (6%)
  other arithmetic  24.1 us (5%)
  between operations  14.3 us (3%)
  local copies, waits for them, and re-layouts  13.4 us (3%)
    reduce_scatter x1, waiting for transfers between devices, shards(): lax.psum_scatter(make_term(saved_rows, grad_proj).astype(jnp.bfloat16), '...  120 us
    all_gather x1, waiting for transfers between devices, shards(): shard_rows = lax.all_gather(weight_both, 'fs', axis=0, tiled=True)  101 us
    psum x1, waiting for transfers between devices, shards(): lax.psum((taps_up_full, taps_gate_full), ('fs', 'tp'))  97.3 us
    reduce_scatter x1, waiting for transfers between devices, shards(): lax.psum_scatter(partial_grad.astype(jnp.bfloat16), 'tp', scatter_dimensi...  29.6 us
    all_gather x1, waiting for transfers between devices, shards(): saved_rows = lax.all_gather(saved_input, 'tp', axis=0, tiled=True)  22.1 us
    unnamed x38, local copies, waits for them, and re-layouts  12.6 us
  transfers between devices with their start and end apart: 6, of which 6 were waited for; matrix products, arithmetic and copies ran while one was open for 11% of the time, Pallas kernels for 0%

commit v1 on v0

--- a/solution.py
+++ b/solution.py
@@ -2,6 +2,14 @@
 import jax.numpy as jnp
 from jax import lax
 from jax.sharding import PartitionSpec as P
+
+
+def measure_views(x_in):
+    mesh_name = "fs"
+    across = "tp"
+    for num in (across, mesh_name):
+        x_in = lax.psum(x_in, axis_name=num)
+    return x_in
 
 
 def delayed(values, steps):
@@ -97,7 +105,7 @@
     taps_gate_full = lax.dynamic_update_slice_in_dim(
         jnp.zeros((3, total_cols), jnp.float32), taps_local[:, column_count:], offset, 1
     )
-    taps_up_total, taps_gate_total = lax.psum((taps_up_full, taps_gate_full), ("fs", "tp"))
+    taps_up_total, taps_gate_total = measure_views((taps_up_full, taps_gate_full))
     weight_grad = lax.psum_scatter(
         make_term(saved_rows, grad_proj).astype(jnp.bfloat16), "fs", scatter_dimension=0, tiled=True
     ).astype(jnp.float32)

time: 460 us -> 441 us (0.959)
  waiting for transfers between devices: 379 us -> 360 us
    psum x1 -> x2, waiting for transfers between devices: 97.3 us -> 79.6 us  [measure_views(): x_in = lax.psum(x_in, axis_name=num)]
  transfers between devices with their start and end apart: 6 -> 7, of which waited for: 6 -> 7; matrix products, arithmetic and copies ran while one was open for 11% -> 11% of each run, Pallas kernels for 0% -> 0%
where the time goes in v1:
time: 441 us; the launch traced here: 440 us
  waiting for transfers between devices  360 us (82%)
  matrix products  28.4 us (6%)
  other arithmetic  24.2 us (5%)
  between operations  14.4 us (3%)
  local copies, waits for them, and re-layouts  13.4 us (3%)
    reduce_scatter x1, waiting for transfers between devices, shards(): lax.psum_scatter(make_term(saved_rows, grad_proj).astype(jnp.bfloat16), '...  118 us
    all_gather x1, waiting for transfers between devices, shards(): shard_rows = lax.all_gather(weight_both, 'fs', axis=0, tiled=True)  101 us
    psum x2, waiting for transfers between devices, measure_views(): x_in = lax.psum(x_in, axis_name=num)  79.6 us
    reduce_scatter x1, waiting for transfers between devices, shards(): lax.psum_scatter(partial_grad.astype(jnp.bfloat16), 'tp', scatter_dimensi...  29.8 us
    all_gather x1, waiting for transfers between devices, shards(): saved_rows = lax.all_gather(saved_input, 'tp', axis=0, tiled=True)  22.1 us
    unnamed x38, local copies, waits for them, and re-layouts  12.6 us
  transfers between devices with their start and end apart: 7, of which 7 were waited for; matrix products, arithmetic and copies ran while one was open for 11% of the time, Pallas kernels for 0%

profile of v1, /device:TPU:0, one launch (start us, length us, event | category | flops | bytes accessed | tf_op | source)
XLA Modules:
  0.0 440.4 jit_solution(17809762040500614578)
XLA Ops:
  7.2 0.7 all-gather.8.cloned.1.call-update
  8.0 2.0 pad_maximum_fusion.1
  10.1 0.7 all-gather.6.cloned.1.call-update
  10.8 1.2 copy.17
  12.0 0.7 constant_dynamic-slice_fusion
  12.8 22.1 %all-gather.8.cloned.1.call-done = bf16[512,2048]{1,0:T(8,128)(2,1)} async-done(((bf16[128,2048]{1,0:T(8,128)(2,1)}), bf16[512,2048]{1,0:T(8,128)(2,1)}) %all-gather.8.cloned.1.call-update) | async-done | bytes 2097168 | tf_op jit(solution)/shard_map/all_gather | solution.py:77
  34.9 101.5 %all-gather.4.cloned.1.call-done = bf16[2048,1536]{1,0:T(8,128)(2,1)} async-done(((bf16[256,1536]{1,0:T(8,128)(2,1)}), bf16[2048,1536]{1,0:T(8,128)(2,1)}) %all-gather.4.cloned.1.call-update) | async-done | bytes 6291472 | tf_op jit(solution)/shard_map/all_gather | solution.py:78
  136.3 6.2 %convert_bitcast_fusion = f32[512,1536]{0,1:T(8,128)S(1)} fusion(bf16[2048,1536]{1,0:T(8,128)(2,1)} %all-gather.4.cloned.1.call-done, bf16[512,2048]{1,0:T(8,128)(2,1)} %all-gather.8.cloned.1.call-done), kind=kOutput, calls=%fused_computation.9 | convolution fusion | flops 3222798336 | bytes 11534336 | tf_op jit(solution)/shard_map/dot_general | solution.py:80
  142.6 2.6 multiply_add_fusion
  145.3 0.9 fusion.4
  146.2 2.8 fusion.1
  149.0 2.6 fusion.2
  151.6 7.1 %all-gather.6.cloned.1.call-done = bf16[512,2048]{1,0:T(8,128)(2,1)} async-done(((bf16[128,2048]{1,0:T(8,128)(2,1)}), bf16[512,2048]{1,0:T(8,128)(2,1)}) %all-gather.6.cloned.1.call-update) | async-done | bytes 2097168 | tf_op jit(solution)/shard_map/all_gather | solution.py:76
  158.7 6.4 %convert_bitcast_fusion.1 = f32[512,1536]{0,1:T(8,128)S(1)} fusion(bf16[2048,1536]{1,0:T(8,128)(2,1)} %all-gather.4.cloned.1.call-done, bf16[512,2048]{1,0:T(8,128)(2,1)} %all-gather.6.cloned.1.call-done), kind=kOutput, calls=%fused_computation.10 | convolution fusion | flops 3222798336 | bytes 11534336 | tf_op jit(solution)/shard_map/dot_general | solution.py:79
  165.1 7.4 %multiply_reduce_fusion.2 = (f32[1536]{0:T(1024)S(1)}, f32[1536]{0:T(1024)S(1)}, f32[1536]{0:T(1024)S(1)}, bf16[512,1536]{0,1:T(8,128)(2,1)}, f32[512,1536]{0,1:T(8,128)}) fusion(f32[510,1536]{0,1:T(8,128)S(1)} %bitcast.20, f32[512,768]{0,1:T(8,128)S(1)} %copy-done.1, f32[512,768]{0,1:T(8,128)S(1)} %copy-done.3, f32[512,1536]{0,1:T(8,128)S(1)} %convert_bitcast_fusion, ...), kind=kLoop, calls=%fused_computation.13 | loop fusion | flops 14151168 | bytes 33011712 | tf_op jit(solution)/shard_map/reduce_sum | solution.py:36
  172.7 0.6 copy-done.13
  173.4 31.8 %all-reduce.13.cloned.1.call-done = (f32[3,3072]{1,0:T(4,128)}, f32[3,3072]{1,0:T(4,128)}) async-done(((f32[3,3072]{1,0:T(4,128)}, f32[3,3072]{1,0:T(4,128)}), (f32[3,3072]{1,0:T(4,128)}, f32[3,3072]{1,0:T(4,128)})) %all-reduce.13.cloned.1.call-update) | async-done | bytes 73744 | tf_op jit(solution)/shard_map/psum | solution.py:11
  205.5 8.2 %fusion = bf16[2048,1536]{0,1:T(8,128)(2,1)} fusion(bf16[512,1536]{0,1:T(8,128)(2,1)} %get-tuple-element.24, bf16[512,2048]{1,0:T(8,128)(2,1)} %all-gather.8.cloned.1.call-done), kind=kOutput, calls=%fused_computation.1 | convolution fusion | flops 3224371200 | bytes 9961472 | tf_op jit(solution)/shard_map/dot_general | solution.py:45
  213.8 1.3 copy-done.10
  215.1 7.6 %convolution_convert_fusion.1 = bf16[512,2048]{1,0:T(8,128)(2,1)} fusion(bf16[512,1536]{0,1:T(8,128)(2,1)S(1)} %copy-done.10, bf16[2048,1536]{1,0:T(8,128)(2,1)} %all-gather.4.cloned.1.call-done), kind=kOutput, calls=%fused_computation.17 | convolution fusion | flops 3222274048 | bytes 9961472 | tf_op jit(solution)/shard_map/dot_general | solution.py:114
  222.7 2.5 copy.19
  225.2 2.3 copy.20
  227.5 1.4 fusion.5
  228.8 2.4 copy.21
  231.2 47.8 %all-reduce.11.cloned.1.call-done = (f32[3,3072]{1,0:T(4,128)}, f32[3,3072]{1,0:T(4,128)}) async-done(((f32[3,3072]{1,0:T(4,128)}, f32[3,3072]{1,0:T(4,128)}), (f32[3,3072]{1,0:T(4,128)}, f32[3,3072]{1,0:T(4,128)})) %all-reduce.11.cloned.1.call-update) | async-done | bytes 73744 | tf_op jit(solution)/shard_map/psum | solution.py:11
  279.0 1.4 multiply_add_fusion.2
  280.5 1.4 multiply_add_fusion.3
  281.9 118.1 %reduce-scatter.5.cloned.1.call-done = bf16[256,1536]{0,1:T(8,128)(2,1)} async-done(((bf16[2048,1536]{0,1:T(8,128)(2,1)}), bf16[256,1536]{0,1:T(8,128)(2,1)}) %reduce-scatter.5.cloned.1.call-update) | async-done | bytes 786448 | tf_op jit(solution)/shard_map/reduce_scatter | solution.py:109
  400.0 1.2 convert_element_type.57
  401.5 1.1 copy.22
  402.7 1.1 copy.23
  403.8 29.8 %reduce-scatter.3.cloned.1.call-done = bf16[128,2048]{1,0:T(8,128)(2,1)} async-done(((bf16[512,2048]{1,0:T(8,128)(2,1)}), bf16[128,2048]{1,0:T(8,128)(2,1)}) %reduce-scatter.3.cloned.1.call-update) | async-done | bytes 524304 | tf_op jit(solution)/shard_map/reduce_scatter | solution.py:120
  (52 shorter events, 1.0 us)
Async XLA Ops:
  7.2 3.7 copy-start.11
  7.2 27.7 %all-gather.8.cloned.1.call-start = ((), (), s32[]{:S(2)}) async-start(), calls=%async_computation.4 | async-start | bytes 2621440 | tf_op jit(solution)/shard_map/all_gather | solution.py:77
  7.9 128.4 %all-gather.4.cloned.1.call-start = ((), (), s32[]{:S(2)}) async-start(), calls=%async_computation.2 | async-start | bytes 7077888 | tf_op jit(solution)/shard_map/all_gather | solution.py:78
  10.0 148.7 %all-gather.6.cloned.1.call-start = ((), (), s32[]{:S(2)}) async-start(), calls=%async_computation.3 | async-start | bytes 2621440 | tf_op jit(solution)/shard_map/all_gather | solution.py:76
  10.8 194.5 %all-reduce.13.cloned.1.call-start = ((), (), s32[]{:S(2)}) async-start(), calls=%async_computation.8 | async-start | bytes 196608 | tf_op jit(solution)/shard_map/psum | solution.py:11
  142.6 2.7 copy-start.9
  146.2 2.8 copy-start
  146.2 2.8 copy-start.2
  158.7 6.4 %copy-start.1 = (f32[512,768]{0,1:T(8,128)S(1)}, f32[512,768]{0,1:T(8,128)}, u32[]{:S(2)}) copy-start(f32[512,768]{0,1:T(8,128)} %copy-done) | copy-start | bytes 4718596
  158.7 6.4 %copy-start.3 = (f32[512,768]{0,1:T(8,128)S(1)}, f32[512,768]{0,1:T(8,128)}, u32[]{:S(2)}) copy-start(f32[512,768]{0,1:T(8,128)} %copy-done.2) | copy-start | bytes 4718596
  158.7 6.4 %copy-start.4 = (f32[511,1536]{0,1:T(8,128)S(1)}, f32[511,1536]{0,1:T(8,128)}, u32[]{:S(2)}) copy-start(f32[511,1536]{0,1:T(8,128)} %fusion.1) | copy-start | bytes 9418756
  158.7 6.4 %copy-start.5 = (f32[510,1536]{0,1:T(8,128)S(1)}, f32[510,1536]{0,1:T(8,128)}, u32[]{:S(2)}) copy-start(f32[510,1536]{0,1:T(8,128)} %fusion.2) | copy-start | bytes 9400324
  172.7 0.6 copy-start.13
  172.7 0.6 copy-start.12
  173.4 105.7 %all-reduce.11.cloned.1.call-start = ((), (), s32[]{:S(2)}) async-start(), calls=%async_computation.7 | async-start | bytes 196608 | tf_op jit(solution)/shard_map/psum | solution.py:11
  205.3 194.8 %reduce-scatter.5.cloned.1.call-start = ((), (), s32[]{:S(2)}) async-start(), calls=%async_computation.6 | async-start | bytes 7077888 | tf_op jit(solution)/shard_map/reduce_scatter | solution.py:109
  213.7 1.4 copy-start.10
  213.7 219.9 %reduce-scatter.3.cloned.1.call-start = ((), (), s32[]{:S(2)}) async-start(), calls=%async_computation.5 | async-start | bytes 2621440 | tf_op jit(solution)/shard_map/reduce_scatter | solution.py:120
  222.7 4.8 %copy-start.6 = (f32[512,1536]{0,1:T(8,128)S(1)}, f32[512,1536]{0,1:T(8,128)}, u32[]{:S(2)}) copy-start(f32[512,1536]{0,1:T(8,128)} %get-tuple-element.27) | copy-start | bytes 9437188
  227.4 51.6 %copy-start.14 = (f32[3,3072]{1,0:T(4,128)S(1)}, f32[3,3072]{1,0:T(4,128)}, u32[]{:S(2)}) copy-start(f32[3,3072]{1,0:T(4,128)} %param.21) | copy-start | bytes 110596
  227.4 53.0 %copy-start.15 = (f32[3,3072]{1,0:T(4,128)S(1)}, f32[3,3072]{1,0:T(4,128)}, u32[]{:S(2)}) copy-start(f32[3,3072]{1,0:T(4,128)} %param.20) | copy-start | bytes 110596
  228.8 172.5 %copy-start.7 = (f32[256,768]{0,1:T(8,128)S(1)}, f32[256,768]{0,1:T(8,128)}, u32[]{:S(2)}) copy-start(f32[256,768]{0,1:T(8,128)} %copy.19) | copy-start | bytes 2359300
  228.8 172.5 %copy-start.8 = (f32[256,768]{0,1:T(8,128)S(1)}, f32[256,768]{0,1:T(8,128)}, u32[]{:S(2)}) copy-start(f32[256,768]{0,1:T(8,128)} %copy.20) | copy-start | bytes 2359300
Sparse Core Ops, SparseCore 0:
  9.5 25.2 all-gather.7
  37.6 98.6 all-gather.3
  137.9 20.7 all-gather.5
  173.5 31.7 all-reduce.12
  208.5 70.4 all-reduce.10
  282.5 117.4 reduce-scatter.4
  403.1 30.4 reduce-scatter.2
